TPU v7x, 32 devices: a whole 2x2x4 slice. The times are simulated.
32 devices in a mesh: sp: 16 (over z, y, x), tp: 2 (over core).
Axes of the slice: x: 2, y: 2, z: 4, core: 2. Of those that a mesh axis runs over, the one named last changes fastest.
Arguments:
- conv_value: bfloat16 [4096, 1024], P('sp', 'tp'), may hold values from -6 to 6
- conv_gate: bfloat16 [4096, 1024], P('sp', 'tp'), may hold values from -6 to 6
- taps: bfloat16 [31, 1024], P(None, 'tp'), may hold values from -1 to 1
- doc_ids: int32 [4096], P('sp'), may hold values from 0 to 3, never falling along the last dimension, each value on 1 to 2048 neighbouring positions
- gn_gain: float32 [1024], P('tp'), may hold values from 0.1 to 1.9
- gn_shift: float32 [1024], P('tp'), may hold values from -3 to 3
- conv_out: bfloat16 [1024, 2048], replicated, may hold values from -0.1875 to 0.1875
- residual: bfloat16 [4096, 2048], P(('sp', 'tp')), may hold values from -6 to 6
- norm_gain: float32 [2048], replicated, may hold values from 0.1 to 1.9
- routes: int32 [4096, 2], P(('sp', 'tp')), may hold values from 0 to 31, as said below
- route_weight: float32 [4096, 2], P(('sp', 'tp')), may hold values from 0.3 to 1.2
- expert_gate: bfloat16 [32, 2048, 512], P(('sp', 'tp')), may hold values from -0.125 to 0.125
- expert_up: bfloat16 [32, 2048, 512], P(('sp', 'tp')), may hold values from -0.125 to 0.125
- expert_down: bfloat16 [32, 512, 2048], P(('sp', 'tp')), may hold values from -0.25 to 0.25
- shared_gate: bfloat16 [2048, 512], replicated, may hold values from -0.125 to 0.125
- shared_up: bfloat16 [2048, 512], replicated, may hold values from -0.125 to 0.125
- shared_down: bfloat16 [512, 2048], replicated, may hold values from -0.25 to 0.25
Outputs:
- layer_out: bfloat16 [4096, 2048], P(('sp', 'tp'))
Inputs may be any that keep to these rules, and one draw needn't show every extreme that they name: `routes`: each row names 2 different experts. The rows of one device name each expert at most 16 times, and one expert, the same for every device, exactly 16 times. `doc_ids`: numbers never fall from one position to the next.
All inputs are finite; a program needn't handle non-finite values.
Results may differ from a plain program's by a relative error of at most 0.014.
Values may be sent and summed in bfloat16 or wider, within the bound.
A program may use at most 128 MiB of HBM per device.

v0:
```python
import jax
import jax.numpy as jnp
from jax import lax
from jax.sharding import PartitionSpec as P

GROUPS = 8
epsilon = 1e-06


def from_behind(x, axis, by):
    peers = lax.axis_size(axis)
    pairs = [(i, i + by) for i in range(peers) if 0 <= i + by < peers]
    return lax.ppermute(x, axis, pairs)


def per_device(
    conv_value,
    conv_gate,
    taps,
    doc_ids,
    gn_gain,
    gn_shift,
    conv_out,
    residual,
    norm_gain,
    routes,
    route_weight,
    expert_gate,
    expert_up,
    expert_down,
    shared_gate,
    shared_up,
    shared_down,
):
    position_count, channel_count = conv_value.shape
    kernel_width = taps.shape[0]
    model_width = residual.shape[1]
    glu_out = (
        conv_value.astype(jnp.float32) * jax.nn.sigmoid(conv_gate.astype(jnp.float32))
    ).astype(jnp.bfloat16)
    rim_start = position_count - kernel_width + 1
    edge_glu, edge_ids = from_behind((glu_out[rim_start:], doc_ids[rim_start:]), "sp", 1)
    longer_glu = jnp.concatenate([edge_glu, glu_out], axis=0)
    longer_ids = jnp.concatenate([edge_ids, doc_ids], axis=0)
    conv_sum = jnp.zeros((position_count, channel_count), jnp.float32)
    for offset in range(kernel_width):
        same_doc = (longer_ids[offset : offset + position_count] == doc_ids)[:, None]
        tap_term = taps[offset].astype(jnp.float32)[None, :] * longer_glu[
            offset : offset + position_count
        ].astype(jnp.float32)
        conv_sum = conv_sum + jnp.where(same_doc, tap_term, 0.0)
    core_split = lax.axis_size("tp")
    groups_here = GROUPS // core_split
    grouped = conv_sum.reshape(position_count, groups_here, channel_count // groups_here)
    group_mean = jnp.mean(grouped, axis=-1, keepdims=True)
    centered = grouped - group_mean
    group_var = jnp.mean(centered * centered, axis=-1, keepdims=True)
    normalized = (centered * lax.rsqrt(group_var + epsilon)).reshape(position_count, channel_count)
    conv_act = jax.nn.silu(normalized * gn_gain + gn_shift).astype(jnp.bfloat16)
    token_rows = lax.all_to_all(conv_act, "tp", split_axis=0, concat_axis=1, tiled=True)
    projected = jnp.dot(token_rows, conv_out, preferred_element_type=jnp.float32)
    stream = (residual.astype(jnp.float32) + projected).astype(jnp.bfloat16)
    stream_wide = stream.astype(jnp.float32)
    normed = (
        stream_wide
        * lax.rsqrt(jnp.mean(stream_wide * stream_wide, axis=-1, keepdims=True) + epsilon)
        * norm_gain
    ).astype(jnp.bfloat16)
    token_count, top_count = routes.shape
    sequence_split = lax.axis_size("sp")
    device_count = sequence_split * core_split
    local_experts = expert_gate.shape[0]
    experts = local_experts * device_count
    capacity = 2 * token_count * top_count // experts
    flat_routes = routes.reshape(-1)
    onehot = (flat_routes[:, None] == jnp.arange(experts, dtype=jnp.int32)[None, :]).astype(
        jnp.int32
    )
    slot_index = jnp.sum(jnp.cumsum(onehot, axis=0) * onehot, axis=1) - 1
    target = flat_routes * capacity + slot_index
    source = (
        jnp.full((experts * capacity,), token_count, jnp.int32)
        .at[target]
        .set(jnp.arange(token_count * top_count, dtype=jnp.int32) // top_count)
    )
    padded_rows = jnp.concatenate([normed, jnp.zeros((1, model_width), normed.dtype)], axis=0)
    outgoing = padded_rows[source]
    shared_hidden = (
        jax.nn.silu(jnp.dot(normed, shared_gate, preferred_element_type=jnp.float32))
        * jnp.dot(normed, shared_up, preferred_element_type=jnp.float32)
    ).astype(jnp.bfloat16)
    shared_out = jnp.dot(shared_hidden, shared_down, preferred_element_type=jnp.float32)
    parcel = outgoing.reshape(device_count, local_experts, capacity, model_width)
    arrived = lax.all_to_all(parcel, ("sp", "tp"), split_axis=0, concat_axis=0, tiled=True)
    expert_rows = arrived[:, 0].reshape(-1, model_width)
    gate_part = jnp.dot(expert_rows, expert_gate[0], preferred_element_type=jnp.float32)
    up_part = jnp.dot(expert_rows, expert_up[0], preferred_element_type=jnp.float32)
    hidden = (jax.nn.silu(gate_part) * up_part).astype(jnp.bfloat16)
    result = jnp.dot(hidden, expert_down[0], preferred_element_type=jnp.float32).astype(
        jnp.bfloat16
    )
    results = [result.reshape(arrived.shape[0], arrived.shape[2], model_width)]
    returned = lax.all_to_all(
        jnp.stack(results, axis=1), ("sp", "tp"), split_axis=0, concat_axis=0, tiled=True
    )
    picked = returned.reshape(experts * capacity, model_width)[target].reshape(
        token_count, top_count, model_width
    )
    routed = jnp.zeros((token_count, model_width), jnp.float32)
    for route_index in range(top_count):
        routed = routed + route_weight[:, route_index, None] * picked[:, route_index].astype(
            jnp.float32
        )
    return (stream_wide + shared_out + routed).astype(jnp.bfloat16)


def solution(mesh):
    return jax.shard_map(
        per_device,
        mesh=mesh,
        in_specs=(
            P("sp", "tp"),
            P("sp", "tp"),
            P(None, "tp"),
            P("sp"),
            P("tp"),
            P("tp"),
            P(),
            P(("sp", "tp"), None),
            P(),
            P(("sp", "tp"), None),
            P(("sp", "tp"), None),
            P(("sp", "tp"), None, None),
            P(("sp", "tp"), None, None),
            P(("sp", "tp"), None, None),
            P(),
            P(),
            P(),
        ),
        out_specs=P(("sp", "tp"), None),
        check_vma=False,
    )
```

profile of v0, /device:TPU:0, one launch (start us, length us, event | category | flops | bytes accessed | tf_op | source)
XLA Modules:
  0.0 168.0 jit_solution(8082973115691364182)
XLA Ops:
  0.0 0.9 slice.297
  0.9 4.9 %collective-permute-start = (s32[30]{0:T(128)S(1)}, s32[30]{0:T(128)S(1)}, u32[]{:S(2)}, u32[]{:S(2)}) collective-permute-start(s32[30]{0:T(128)S(1)} %slice.297), channel_id=1, source_target_pairs={{0,2},{2,4},{4,6},{6,8},{8,10},{10,12},{12,14},{14,16},{16,18},{18... | collective-permute-start | bytes 368 | tf_op jit(solution)/shard_map/ppermute | solution.py:13
  5.8 1.2 multiply_convert_fusion.2
  7.0 3.4 %collective-permute-start.1 = (bf16[30,512]{1,0:T(8,128)(2,1)S(1)}, bf16[30,512]{1,0:T(8,128)(2,1)S(1)}, u32[]{:S(2)}, u32[]{:S(2)}) collective-permute-start(bf16[30,512]{1,0:T(8,128)(2,1)S(1)} %slice.400), channel_id=1, source_target_pairs={{0,2},{2,4},{4,6},{6,8},{8,10},{10,12},{12,14},{14,16},{16,18},{18... | collective-permute-start | bytes 92168 | tf_op jit(solution)/shard_map/ppermute | solution.py:13
  10.4 1.0 slice_convert_fusion.30
  11.4 1.0 slice_convert_fusion.29
  12.4 0.8 copy.33
  13.5 0.7 broadcast_multiply_fusion.1
  14.2 0.6 reduce-window.6
  15.4 1.4 scatter_custom_fusion
  16.8 0.8 pad_add_fusion
  17.6 0.8 slice_compare_fusion.29
  18.4 0.8 slice_compare_fusion.28
  19.1 4.0 %multiply_add_fusion = f32[256,512]{1,0:T(8,128)S(1)} fusion(bf16[256,512]{1,0:T(8,128)(2,1)S(1)} %multiply_convert_fusion.2, bf16[30,512]{1,0:T(8,128)(2,1)S(1)} %collective-permute-done.1, f32[512]{0:T(512)S(1)} %bitcast.151, f32[512]{0:T(512)S(1)} %bitcast.152, f32[512]{0:T(512)S(1)} %bitcast.123, f32[512]{0:T(512)S(1)} %bitcast.124, ...), kind=kLoop, calls=%fused_computation.62 | loop fusion | flops 27787264 | bytes 888320 | tf_op jit(solution)/shard_map/add | solution.py:51
  23.4 0.3 reduce_sum.36
  23.8 0.6 multiply_reduce_fusion.1
  24.8 0.3 sub.25
  25.3 3.9 %all_to_all.29 = bf16[2,128,512]{2,1,0:T(8,128)(2,1)S(1)} all-to-all(bf16[2,128,512]{2,1,0:T(8,128)(2,1)S(1)} %bitcast.119), channel_id=1, replica_groups=mesh['sp'=16,'tp'=2] {'tp'}, dimensions={0} | all-to-all | bytes 524288 | tf_op jit(solution)/shard_map/all_to_all | solution.py:60
  29.5 3.0 %multiply_reduce_fusion = (f32[128]{0:T(128)S(1)}, f32[128,2048]{1,0:T(8,128)S(1)}) fusion(bf16[128,1024]{0,1:T(8,128)(2,1)S(1)} %bitcast.120, bf16[1024,2048]{1,0:T(8,128)(2,1)} %param.23, bf16[128,2048]{1,0:T(8,128)(2,1)S(1)} %copy-done.4), kind=kOutput, calls=%fused_computation.52 | convolution fusion | flops 538443648 | bytes 6029824 | tf_op jit(solution)/shard_map/dot_general | solution.py:61
  32.5 1.0 copy-done.2
  33.7 3.3 %gather_fusion = bf16[512,2048]{1,0:T(8,128)(2,1)} fusion(bf16[129,2048]{1,0:T(8,128)(2,1)S(1)} %concatenate.11, s32[1024]{0:T(1024)S(1)} %pad_clamp_fusion.1), kind=kCustom, calls=%fused_computation | custom fusion | bytes 4196352 | tf_op jit(solution)/shard_map/gather | solution.py:87
  37.1 53.6 %all_to_all.30 = bf16[32,1,16,2048]{3,2,1,0:T(8,128)(2,1)S(1)} all-to-all(bf16[32,1,16,2048]{3,2,1,0:T(8,128)(2,1)} %bitcast.113), channel_id=1, replica_groups=mesh['sp'=16,'tp'=2] {'sp','tp'}, dimensions={0} | all-to-all | bytes 4194304 | tf_op jit(solution)/shard_map/all_to_all | solution.py:94
  90.6 1.3 copy-done.3
  91.9 2.3 %fusion.7 = f32[512,512]{1,0:T(8,128)} fusion(bf16[512,2048]{1,0:T(8,128)(2,1)S(1)} %bitcast.117, bf16[1,2048,512]{2,1,0:T(8,128)(2,1)S(1)} %copy-done.9), kind=kOutput, calls=%fused_computation.42 | convolution fusion | flops 1073741824 | bytes 5242880 | tf_op jit(solution)/shard_map/dot_general | solution.py:96
  94.2 6.3 %convolution_convert_fusion = bf16[512,2048]{1,0:T(8,128)(2,1)} fusion(bf16[1,512,2048]{2,1,0:T(8,128)(2,1)S(1)} %copy-done, bf16[512,2048]{1,0:T(8,128)(2,1)} %bitcast.118, bf16[1,2048,512]{2,1,0:T(8,128)(2,1)} %param.29, f32[512,512]{1,0:T(8,128)} %fusion.7), kind=kOutput, calls=%fused_computation.3 | convolution fusion | flops 2150105088 | bytes 9437184 | tf_op jit(solution)/shard_map/dot_general | solution.py:99
  100.5 4.0 %all-to-all-start.2 = ((bf16[32,1,16,2048]{3,2,1,0:T(8,128)(2,1)}), bf16[32,1,16,2048]{3,2,1,0:T(8,128)(2,1)}, u32[]{:S(2)}, u32[]{:S(2)}) async-start(bf16[32,1,16,2048]{3,2,1,0:T(8,128)(2,1)} %bitcast.116), calls=%async_computation.2 | async-start | bytes 4194304 | tf_op jit(solution)/shard_map/all_to_all | solution.py:103
  104.5 2.0 %fusion.65 = f32[128,512]{1,0:T(8,128)S(1)} fusion(bf16[128,2048]{1,0:T(8,128)(2,1)S(1)} %multiply_convert_fusion, bf16[2048,512]{1,0:T(8,128)(2,1)} %param.31), kind=kOutput, calls=%fused_computation.198 | convolution fusion | flops 268435456 | bytes 2883584 | tf_op jit(solution)/shard_map/dot_general | solution.py:89
  106.5 46.6 %all-to-all-done.2 = bf16[32,1,16,2048]{3,2,1,0:T(8,128)(2,1)} async-done(((bf16[32,1,16,2048]{3,2,1,0:T(8,128)(2,1)}), bf16[32,1,16,2048]{3,2,1,0:T(8,128)(2,1)}, u32[]{:S(2)}, u32[]{:S(2)}) %all-to-all-start.2) | async-done | bytes 2097184 | tf_op jit(solution)/shard_map/all_to_all | solution.py:103
  153.1 5.2 %gather_fusion.1 = bf16[256,2048]{1,0:T(8,128)(2,1)} fusion(bf16[512,2048]{1,0:T(8,128)(2,1)} %bitcast.46, s32[1024]{0:T(1024)S(1)} %pad_clamp_fusion), kind=kCustom, calls=%fused_computation.1 | custom fusion | bytes 2098176 | tf_op jit(solution)/shard_map/gather | solution.py:106
  158.3 1.7 %reshape.130 = bf16[128,2,2048]{2,1,0:T(2,128)(2,1)S(1)} reshape(bf16[256,2048]{1,0:T(8,128)(2,1)} %gather_fusion.1) | data formatting | bytes 2097152 | tf_op jit(solution)/shard_map/reshape | solution.py:106
  160.1 2.5 %fusion.64 = (bf16[128,1,2048]{2,1,0:T(2,128)(2,1)}, bf16[128,1,2048]{2,1,0:T(2,128)(2,1)}) fusion(bf16[128,2,2048]{2,1,0:T(2,128)(2,1)S(1)} %reshape.130), kind=kLoop, calls=%fused_computation.197 | loop fusion | bytes 2097152 | tf_op jit(solution)/shard_map/slice | solution.py:111
  162.6 5.4 %fusion.3 = bf16[128,2048]{1,0:T(8,128)(2,1)} fusion(f32[128,2048]{1,0:T(8,128)} %copy-done.2, bf16[512,2048]{1,0:T(8,128)(2,1)} %param.33, bf16[128,2048]{1,0:T(8,128)(2,1)} %copy-done.1, bf16[2048,512]{1,0:T(8,128)(2,1)} %param.32, bf16[128,1,2048]{2,1,0:T(2,128)(2,1)} %get-tuple-element.6, bf16[128,1,2048]{2,1,0:T(2,128)(2,1)} %get-tuple-element.5, ...), kind=kOutput, calls=%fused_computation.38 | convolution fusion | flops 539361280 | bytes 7603200 | tf_op jit(solution)/shard_map/dot_general | solution.py:92
  (46 shorter events, 2.1 us)
Async XLA Ops:
  0.0 94.2 %copy-start = (bf16[1,512,2048]{2,1,0:T(8,128)(2,1)S(1)}, bf16[1,512,2048]{2,1,0:T(8,128)(2,1)}, u32[]{:S(2)}) copy-start(bf16[1,512,2048]{2,1,0:T(8,128)(2,1)} %param.30) | copy-start | bytes 6291460
  0.9 15.9 %collective-permute-start = (s32[30]{0:T(128)S(1)}, s32[30]{0:T(128)S(1)}, u32[]{:S(2)}, u32[]{:S(2)}) collective-permute-start(s32[30]{0:T(128)S(1)} %slice.297), channel_id=1, source_target_pairs={{0,2},{2,4},{4,6},{6,8},{8,10},{10,12},{12,14},{14,16},{16,18},{18... | collective-permute-start | bytes 368 | tf_op jit(solution)/shard_map/ppermute | solution.py:13
  7.0 12.2 %collective-permute-start.1 = (bf16[30,512]{1,0:T(8,128)(2,1)S(1)}, bf16[30,512]{1,0:T(8,128)(2,1)S(1)}, u32[]{:S(2)}, u32[]{:S(2)}) collective-permute-start(bf16[30,512]{1,0:T(8,128)(2,1)S(1)} %slice.400), channel_id=1, source_target_pairs={{0,2},{2,4},{4,6},{6,8},{8,10},{10,12},{12,14},{14,16},{16,18},{18... | collective-permute-start | bytes 92168 | tf_op jit(solution)/shard_map/ppermute | solution.py:13
  23.2 1.9 %copy-start.6 = (f32[512]{0:T(512)S(1)}, f32[512]{0:T(512)}, u32[]{:S(2)}) copy-start(f32[512]{0:T(512)} %param.22) | copy-start | bytes 6148
  23.2 1.9 %copy-start.7 = (f32[512]{0:T(512)S(1)}, f32[512]{0:T(512)}, u32[]{:S(2)}) copy-start(f32[512]{0:T(512)} %param.21) | copy-start | bytes 6148
  24.4 5.0 %copy-start.4 = (bf16[128,2048]{1,0:T(8,128)(2,1)S(1)}, bf16[128,2048]{1,0:T(8,128)(2,1)}, u32[]{:S(2)}) copy-start(bf16[128,2048]{1,0:T(8,128)(2,1)} %param.24) | copy-start | bytes 1572868
  29.5 4.0 %copy-start.5 = (f32[2048]{0:T(1024)S(1)}, f32[2048]{0:T(1024)}, u32[]{:S(2)}) copy-start(f32[2048]{0:T(1024)} %param.25) | copy-start | bytes 24580
  32.5 1.0 copy-start.2
  33.6 70.8 %copy-start.1 = (bf16[128,2048]{1,0:T(8,128)(2,1)}, bf16[128,2048]{1,0:T(8,128)(2,1)S(1)}, u32[]{:S(2)}) copy-start(bf16[128,2048]{1,0:T(8,128)(2,1)S(1)} %multiply_convert_fusion) | copy-start | bytes 1572868
  37.1 54.9 %copy-start.9 = (bf16[1,2048,512]{2,1,0:T(8,128)(2,1)S(1)}, bf16[1,2048,512]{2,1,0:T(8,128)(2,1)}, u32[]{:S(2)}) copy-start(bf16[1,2048,512]{2,1,0:T(8,128)(2,1)} %param.28) | copy-start | bytes 6291460
  90.6 1.3 copy-start.3
  100.5 4.0 %copy-start.8 = (f32[128,2]{0,1:T(2,128)S(1)}, f32[128,2]{0,1:T(2,128)}, u32[]{:S(2)}) copy-start(f32[128,2]{0,1:T(2,128)} %param.27) | copy-start | bytes 3076
  100.5 52.6 %all-to-all-start.2 = ((bf16[32,1,16,2048]{3,2,1,0:T(8,128)(2,1)}), bf16[32,1,16,2048]{3,2,1,0:T(8,128)(2,1)}, u32[]{:S(2)}, u32[]{:S(2)}) async-start(bf16[32,1,16,2048]{3,2,1,0:T(8,128)(2,1)} %bitcast.116), calls=%async_computation.2 | async-start | bytes 4194304 | tf_op jit(solution)/shard_map/all_to_all | solution.py:103
where the time goes:
time: 169 us; the launch traced here: 168 us
  blocking collectives  57.5 us (34%)
  waiting for transfers between devices  46.6 us (28%)
  local copies, waits for them, and re-layouts  20 us (12%)
  matrix products  19 us (11%)
  other arithmetic  12.3 us (7%)
  starting transfers between devices  12.2 us (7%)
    all_to_all x1, blocking collectives, per_device(): lax.all_to_all(parcel, ('sp', 'tp'), split_axis=0, concat_axis=0, tiled=T...  53.6 us
    all_to_all x1, waiting for transfers between devices, per_device(): lax.all_to_all(jnp.stack(results, axis=1), ('sp', 'tp'), split_axis=0, co...  46.6 us
    ppermute x2, starting transfers between devices, from_behind(): return lax.ppermute(x, axis, pairs)  8.26 us
    dot_general x1, matrix products, per_device(): jnp.dot(hidden, expert_down[0], preferred_element_type=jnp.float32)  6.28 us
    dot_general x1, matrix products, per_device(): jnp.dot(shared_hidden, shared_down, preferred_element_type=jnp.float32)  5.43 us
    gather x1, local copies, waits for them, and re-layouts, per_device(): returned.reshape(experts * capacity, model_width)[target]  5.21 us
    add x1, other arithmetic, per_device(): conv_sum = conv_sum + jnp.where(same_doc, tap_term, 0.0)  4.03 us
    all_to_all x1, starting transfers between devices, per_device(): lax.all_to_all(jnp.stack(results, axis=1), ('sp', 'tp'), split_axis=0, co...  3.96 us
  transfers between devices with their start and end apart: 3, of which 1 were waited for; matrix products, arithmetic and copies ran while one was open for 7% of the time, Pallas kernels for 0%

commit v1 on v0

--- a/solution.py
+++ b/solution.py
@@ -57,7 +57,13 @@
     group_var = jnp.mean(centered * centered, axis=-1, keepdims=True)
     normalized = (centered * lax.rsqrt(group_var + epsilon)).reshape(position_count, channel_count)
     conv_act = jax.nn.silu(normalized * gn_gain + gn_shift).astype(jnp.bfloat16)
-    token_rows = lax.all_to_all(conv_act, "tp", split_axis=0, concat_axis=1, tiled=True)
+    arrays_proceed = lambda sheet, axis_tag, axis_k, in_dim: jnp.concatenate(
+        lax.all_to_all(
+            jnp.stack(jnp.split(sheet, lax.axis_size(axis_tag), axis=axis_k)), axis_tag, 0, 0
+        ),
+        axis=in_dim,
+    )
+    token_rows = arrays_proceed(conv_act, "tp", 0, 1)
     projected = jnp.dot(token_rows, conv_out, preferred_element_type=jnp.float32)
     stream = (residual.astype(jnp.float32) + projected).astype(jnp.bfloat16)
     stream_wide = stream.astype(jnp.float32)

time: 169 us -> 166 us (0.982)
  other arithmetic: 12.3 us -> 8.06 us
    reduce_sum x1, other arithmetic: 0.34 us -> 6.33 us  [per_device(): group_mean = jnp.mean(grouped, axis=-1, keepdims=True)]
    add x1 -> x0, other arithmetic: 4.03 us -> none  [per_device(): conv_sum = conv_sum + jnp.where(same_doc, tap_term, 0.0)]
    mul x2, other arithmetic: 2.02 us -> 0.05 us  [per_device(): taps[offset].astype(jnp.float32)[None, :]]
    unnamed x21 -> x29, local copies, waits for them, and re-layouts: 3.09 us -> 4.61 us
  transfers between devices with their start and end apart: 3 -> 3, of which waited for: 1 -> 1; matrix products, arithmetic and copies ran while one was open for 7% -> 5% of each run, Pallas kernels for 0% -> 0%
where the time goes in v1:
time: 166 us; the launch traced here: 165 us
  blocking collectives  58.3 us (35%)
  waiting for transfers between devices  46.6 us (28%)
  local copies, waits for them, and re-layouts  20.5 us (12%)
  matrix products  19 us (11%)
  starting transfers between devices  12.2 us (7%)
  other arithmetic  8.06 us (5%)
    all_to_all x1, blocking collectives, per_device(): lax.all_to_all(parcel, ('sp', 'tp'), split_axis=0, concat_axis=0, tiled=T...  54.3 us
    all_to_all x1, waiting for transfers between devices, per_device(): lax.all_to_all(jnp.stack(results, axis=1), ('sp', 'tp'), split_axis=0, co...  46.6 us
    ppermute x2, starting transfers between devices, from_behind(): return lax.ppermute(x, axis, pairs)  8.27 us
    reduce_sum x1, other arithmetic, per_device(): group_mean = jnp.mean(grouped, axis=-1, keepdims=True)  6.33 us
    dot_general x1, matrix products, per_device(): jnp.dot(hidden, expert_down[0], preferred_element_type=jnp.float32)  6.25 us
    dot_general x1, matrix products, per_device(): jnp.dot(shared_hidden, shared_down, preferred_element_type=jnp.float32)  5.43 us
    gather x1, local copies, waits for them, and re-layouts, per_device(): returned.reshape(experts * capacity, model_width)[target]  5.19 us
    unnamed x29, local copies, waits for them, and re-layouts  4.61 us
  transfers between devices with their start and end apart: 3, of which 1 were waited for; matrix products, arithmetic and copies ran while one was open for 5% of the time, Pallas kernels for 0%

profile of v1, /device:TPU:0, one launch (start us, length us, event | category | flops | bytes accessed | tf_op | source)
XLA Modules:
  0.0 165.1 jit_solution(3022685406008928230)
XLA Ops:
  0.0 0.9 slice.297
  0.9 4.9 %collective-permute-start = (s32[30]{0:T(128)S(1)}, s32[30]{0:T(128)S(1)}, u32[]{:S(2)}, u32[]{:S(2)}) collective-permute-start(s32[30]{0:T(128)S(1)} %slice.297), channel_id=1, source_target_pairs={{0,2},{2,4},{4,6},{6,8},{8,10},{10,12},{12,14},{14,16},{16,18},{18... | collective-permute-start | bytes 368 | tf_op jit(solution)/shard_map/ppermute | solution.py:13
  5.8 1.1 copy.26
  6.9 1.1 copy.27
  8.0 0.2 multiply_convert_fusion.2
  8.3 3.4 %collective-permute-start.1 = (bf16[30,512]{0,1:T(8,128)(2,1)S(1)}, bf16[30,512]{0,1:T(8,128)(2,1)S(1)}, u32[]{:S(2)}, u32[]{:S(2)}) collective-permute-start(bf16[30,512]{0,1:T(8,128)(2,1)S(1)} %slice.400), channel_id=1, source_target_pairs={{0,2},{2,4},{4,6},{6,8},{8,10},{10,12},{12,14},{14,16},{16,18},{18... | collective-permute-start | bytes 92168 | tf_op jit(solution)/shard_map/ppermute | solution.py:13
  11.8 0.1 copy.29
  11.9 0.1 eq.149
  12.0 0.1 eq.145
  12.2 0.6 reduce-window.6
  12.8 0.2 slice_reduce_fusion
  13.1 0.1 copy.28
  13.2 0.1 mul.647
  13.4 1.4 scatter_custom_fusion
  15.1 6.3 %bitcast_reduce_fusion = (f32[256,4]{0,1:T(4,128)S(1)}, f32[256,512]{0,1:T(8,128)S(1)}) fusion(bf16[256,512]{0,1:T(8,128)(2,1)S(1)} %multiply_convert_fusion.2, f32[512]{0:T(512)S(1)} %bitcast.156, bf16[30,512]{0,1:T(8,128)(2,1)S(1)} %collective-permute-done.1, f32[512]{0:T(512)S(1)} %bitcast.157, pred[256]{0:T(512)(128)(4,1)S(1)} %get-tuple-element.70, ...), kind=kLoop, calls=%fused_computation.89 | loop fusion | flops 27917312 | bytes 892416 | tf_op jit(solution)/shard_map/reduce_sum | solution.py:55
  21.6 0.2 multiply_convert_fusion.1
  21.9 3.9 %all_to_all.15 = bf16[2,128,512]{1,2,0:T(8,128)(2,1)S(1)} all-to-all(bf16[2,128,512]{1,2,0:T(8,128)(2,1)S(1)} %pad_maximum_fusion.1), channel_id=1, replica_groups=mesh['sp'=16,'tp'=2] {'tp'}, dimensions={0} | all-to-all | bytes 524288 | tf_op jit(solution)/shard_map/all_to_all | solution.py:61
  25.9 3.0 %multiply_reduce_fusion = (f32[128]{0:T(128)S(1)}, f32[128,2048]{1,0:T(8,128)S(1)}) fusion(bf16[128,1024]{0,1:T(8,128)(2,1)S(1)} %bitcast.126, bf16[1024,2048]{1,0:T(8,128)(2,1)} %param.23, bf16[128,2048]{1,0:T(8,128)(2,1)S(1)} %copy-done.4), kind=kOutput, calls=%fused_computation.52 | convolution fusion | flops 538443648 | bytes 6029824 | tf_op jit(solution)/shard_map/dot_general | solution.py:67
  28.9 1.0 copy-done.2
  29.9 0.2 multiply_convert_fusion
  30.1 3.3 %gather_fusion = bf16[512,2048]{1,0:T(8,128)(2,1)} fusion(bf16[129,2048]{1,0:T(8,128)(2,1)S(1)} %concatenate.11, s32[1024]{0:T(1024)S(1)} %pad_clamp_fusion.1), kind=kCustom, calls=%fused_computation | custom fusion | bytes 4196352 | tf_op jit(solution)/shard_map/gather | solution.py:93
  33.4 54.3 %all_to_all.16 = bf16[32,1,16,2048]{3,2,1,0:T(8,128)(2,1)S(1)} all-to-all(bf16[32,1,16,2048]{3,2,1,0:T(8,128)(2,1)} %bitcast.122), channel_id=1, replica_groups=mesh['sp'=16,'tp'=2] {'sp','tp'}, dimensions={0} | all-to-all | bytes 4194304 | tf_op jit(solution)/shard_map/all_to_all | solution.py:100
  87.8 1.3 copy-done.3
  89.1 2.2 %fusion.7 = f32[512,512]{1,0:T(8,128)} fusion(bf16[512,2048]{1,0:T(8,128)(2,1)S(1)} %bitcast.124, bf16[1,2048,512]{2,1,0:T(8,128)(2,1)S(1)} %copy-done.12), kind=kOutput, calls=%fused_computation.42 | convolution fusion | flops 1073741824 | bytes 5242880 | tf_op jit(solution)/shard_map/dot_general | solution.py:102
  91.3 6.2 %convolution_convert_fusion = bf16[512,2048]{1,0:T(8,128)(2,1)} fusion(bf16[1,512,2048]{2,1,0:T(8,128)(2,1)S(1)} %copy-done, bf16[512,2048]{1,0:T(8,128)(2,1)} %bitcast.125, bf16[1,2048,512]{2,1,0:T(8,128)(2,1)} %param.29, f32[512,512]{1,0:T(8,128)} %fusion.7), kind=kOutput, calls=%fused_computation.3 | convolution fusion | flops 2150105088 | bytes 9437184 | tf_op jit(solution)/shard_map/dot_general | solution.py:105
  97.6 4.0 %all-to-all-start.2 = ((bf16[32,1,16,2048]{3,2,1,0:T(8,128)(2,1)}), bf16[32,1,16,2048]{3,2,1,0:T(8,128)(2,1)}, u32[]{:S(2)}, u32[]{:S(2)}) async-start(bf16[32,1,16,2048]{3,2,1,0:T(8,128)(2,1)} %bitcast.123), calls=%async_computation.2 | async-start | bytes 4194304 | tf_op jit(solution)/shard_map/all_to_all | solution.py:109
  101.6 2.0 %fusion.67 = f32[128,512]{1,0:T(8,128)S(1)} fusion(bf16[128,2048]{1,0:T(8,128)(2,1)S(1)} %multiply_convert_fusion, bf16[2048,512]{1,0:T(8,128)(2,1)} %param.31), kind=kOutput, calls=%fused_computation.225 | convolution fusion | flops 268435456 | bytes 2883584 | tf_op jit(solution)/shard_map/dot_general | solution.py:95
  103.7 46.6 %all-to-all-done.2 = bf16[32,1,16,2048]{3,2,1,0:T(8,128)(2,1)} async-done(((bf16[32,1,16,2048]{3,2,1,0:T(8,128)(2,1)}), bf16[32,1,16,2048]{3,2,1,0:T(8,128)(2,1)}, u32[]{:S(2)}, u32[]{:S(2)}) %all-to-all-start.2) | async-done | bytes 2097184 | tf_op jit(solution)/shard_map/all_to_all | solution.py:109
  150.2 5.2 %gather_fusion.1 = bf16[256,2048]{1,0:T(8,128)(2,1)} fusion(bf16[512,2048]{1,0:T(8,128)(2,1)} %bitcast.50, s32[1024]{0:T(1024)S(1)} %pad_clamp_fusion), kind=kCustom, calls=%fused_computation.1 | custom fusion | bytes 2098176 | tf_op jit(solution)/shard_map/gather | solution.py:112
  155.4 1.7 %reshape.135 = bf16[128,2,2048]{2,1,0:T(2,128)(2,1)S(1)} reshape(bf16[256,2048]{1,0:T(8,128)(2,1)} %gather_fusion.1) | data formatting | bytes 2097152 | tf_op jit(solution)/shard_map/reshape | solution.py:112
  157.2 2.5 %fusion.66 = (bf16[128,1,2048]{2,1,0:T(2,128)(2,1)}, bf16[128,1,2048]{2,1,0:T(2,128)(2,1)}) fusion(bf16[128,2,2048]{2,1,0:T(2,128)(2,1)S(1)} %reshape.135), kind=kLoop, calls=%fused_computation.224 | loop fusion | bytes 2097152 | tf_op jit(solution)/shard_map/slice | solution.py:117
  159.6 5.4 %fusion.3 = bf16[128,2048]{1,0:T(8,128)(2,1)} fusion(f32[128,2048]{1,0:T(8,128)} %copy-done.2, bf16[512,2048]{1,0:T(8,128)(2,1)} %param.33, bf16[128,2048]{1,0:T(8,128)(2,1)} %copy-done.1, bf16[2048,512]{1,0:T(8,128)(2,1)} %param.32, bf16[128,1,2048]{2,1,0:T(2,128)(2,1)} %get-tuple-element.8, bf16[128,1,2048]{2,1,0:T(2,128)(2,1)} %get-tuple-element.7, ...), kind=kOutput, calls=%fused_computation.38 | convolution fusion | flops 539361280 | bytes 7603200 | tf_op jit(solution)/shard_map/dot_general | solution.py:98
  (51 shorter events, 0.8 us)
Async XLA Ops:
  0.0 91.3 %copy-start = (bf16[1,512,2048]{2,1,0:T(8,128)(2,1)S(1)}, bf16[1,512,2048]{2,1,0:T(8,128)(2,1)}, u32[]{:S(2)}) copy-start(bf16[1,512,2048]{2,1,0:T(8,128)(2,1)} %param.30) | copy-start | bytes 6291460
  0.0 14.9 %copy-start.6 = (s32[256]{0:T(256)S(1)}, s32[256]{0:T(256)}, u32[]{:S(2)}) copy-start(s32[256]{0:T(256)} %param.20) | copy-start | bytes 3076
  0.0 11.7 %copy-start.5 = (bf16[31,512]{1,0:T(8,128)(2,1)S(1)}, bf16[31,512]{1,0:T(8,128)(2,1)}, u32[]{:S(2)}) copy-start(bf16[31,512]{1,0:T(8,128)(2,1)} %param.19) | copy-start | bytes 95236
  0.0 11.8 %copy-start.8 = (s32[128,2]{0,1:T(2,128)S(1)}, s32[128,2]{0,1:T(2,128)}, u32[]{:S(2)}) copy-start(s32[128,2]{0,1:T(2,128)} %param.26) | copy-start | bytes 3076
  0.9 13.9 %collective-permute-start = (s32[30]{0:T(128)S(1)}, s32[30]{0:T(128)S(1)}, u32[]{:S(2)}, u32[]{:S(2)}) collective-permute-start(s32[30]{0:T(128)S(1)} %slice.297), channel_id=1, source_target_pairs={{0,2},{2,4},{4,6},{6,8},{8,10},{10,12},{12,14},{14,16},{16,18},{18... | collective-permute-start | bytes 368 | tf_op jit(solution)/shard_map/ppermute | solution.py:13
  6.9 14.7 %copy-start.9 = (f32[512]{0:T(512)S(1)}, f32[512]{0:T(512)}, u32[]{:S(2)}) copy-start(f32[512]{0:T(512)} %param.22) | copy-start | bytes 6148
  6.9 14.7 %copy-start.10 = (f32[512]{0:T(512)S(1)}, f32[512]{0:T(512)}, u32[]{:S(2)}) copy-start(f32[512]{0:T(512)} %param.21) | copy-start | bytes 6148
  8.3 6.9 %collective-permute-start.1 = (bf16[30,512]{0,1:T(8,128)(2,1)S(1)}, bf16[30,512]{0,1:T(8,128)(2,1)S(1)}, u32[]{:S(2)}, u32[]{:S(2)}) collective-permute-start(bf16[30,512]{0,1:T(8,128)(2,1)S(1)} %slice.400), channel_id=1, source_target_pairs={{0,2},{2,4},{4,6},{6,8},{8,10},{10,12},{12,14},{14,16},{16,18},{18... | collective-permute-start | bytes 92168 | tf_op jit(solution)/shard_map/ppermute | solution.py:13
  13.4 12.5 %copy-start.4 = (bf16[128,2048]{1,0:T(8,128)(2,1)S(1)}, bf16[128,2048]{1,0:T(8,128)(2,1)}, u32[]{:S(2)}) copy-start(bf16[128,2048]{1,0:T(8,128)(2,1)} %param.24) | copy-start | bytes 1572868
  25.9 4.0 %copy-start.7 = (f32[2048]{0:T(1024)S(1)}, f32[2048]{0:T(1024)}, u32[]{:S(2)}) copy-start(f32[2048]{0:T(1024)} %param.25) | copy-start | bytes 24580
  28.9 1.0 copy-start.2
  30.0 71.6 %copy-start.1 = (bf16[128,2048]{1,0:T(8,128)(2,1)}, bf16[128,2048]{1,0:T(8,128)(2,1)S(1)}, u32[]{:S(2)}) copy-start(bf16[128,2048]{1,0:T(8,128)(2,1)S(1)} %multiply_convert_fusion) | copy-start | bytes 1572868
  33.4 55.7 %copy-start.12 = (bf16[1,2048,512]{2,1,0:T(8,128)(2,1)S(1)}, bf16[1,2048,512]{2,1,0:T(8,128)(2,1)}, u32[]{:S(2)}) copy-start(bf16[1,2048,512]{2,1,0:T(8,128)(2,1)} %param.28) | copy-start | bytes 6291460
  87.8 1.3 copy-start.3
  97.6 4.0 %copy-start.11 = (f32[128,2]{0,1:T(2,128)S(1)}, f32[128,2]{0,1:T(2,128)}, u32[]{:S(2)}) copy-start(f32[128,2]{0,1:T(2,128)} %param.27) | copy-start | bytes 3076
  97.6 52.6 %all-to-all-start.2 = ((bf16[32,1,16,2048]{3,2,1,0:T(8,128)(2,1)}), bf16[32,1,16,2048]{3,2,1,0:T(8,128)(2,1)}, u32[]{:S(2)}, u32[]{:S(2)}) async-start(bf16[32,1,16,2048]{3,2,1,0:T(8,128)(2,1)} %bitcast.123), calls=%async_computation.2 | async-start | bytes 4194304 | tf_op jit(solution)/shard_map/all_to_all | solution.py:109
